TPU v7x, 512 devices: a whole 4x8x8 slice. The times are simulated.
512 devices in a mesh: sp: 32 (over z, x), tp: 16 (over y, core).
Axes of the slice: x: 4, y: 8, z: 8, core: 2. Of those that a mesh axis runs over, the one named last changes fastest.
Arguments:
- resid: bfloat16 [4096, 2048], P('sp'), may hold values from -8 to 8
- a_val: bfloat16 [4096, 1024], P('sp', 'tp'), may hold values from -8 to 8
- a_gate: bfloat16 [4096, 1024], P('sp', 'tp'), may hold values from -6 to 6
- conv_kernel: bfloat16 [31, 1024], P(None, 'tp'), may hold values from -1 to 1
- conv_bias: float32 [1024], P('tp'), may hold values from -3 to 3
- ln_gain: float32 [1024], P('tp'), may hold values from 0.1 to 1.9
- ln_bias: float32 [1024], P('tp'), may hold values from -3 to 3
- w_out: bfloat16 [1024, 2048], P('tp'), may hold values from -0.1875 to 0.1875
- ffn_gain: float32 [2048], replicated, may hold values from 0.1 to 1.9
- routes: int32 [4096, 4], P('sp'), may hold values from 0 to 31, all different within a row; in each aligned block of 128 rows (0 to 127, 128 to 255, ...) at most 32 rows name the same one
- route_weights: float32 [4096, 4], P('sp'), may hold values from 0.15 to 1.2
- exp_gate: bfloat16 [32, 2048, 4096], P('sp', None, 'tp'), may hold values from -0.125 to 0.125
- exp_up: bfloat16 [32, 2048, 4096], P('sp', None, 'tp'), may hold values from -0.125 to 0.125
- exp_down: bfloat16 [32, 4096, 2048], P('sp', None, 'tp'), may hold values from -0.09375 to 0.09375
- sh_gate: bfloat16 [2048, 512], P(None, 'tp'), may hold values from -0.125 to 0.125
- sh_up: bfloat16 [2048, 512], P(None, 'tp'), may hold values from -0.125 to 0.125
- sh_down: bfloat16 [512, 2048], P(None, 'tp'), may hold values from -0.25 to 0.25
Outputs:
- result: bfloat16 [4096, 2048], P('sp', 'tp')
Inputs may be any that keep to these rules, and one draw needn't show every extreme that they name: `routes`: among the 128 rows of one index of sp, each expert is named at most 32 times, a bound that some block reaches; a row names 4 different experts.
All inputs are finite; a program needn't handle non-finite values.
Results may differ from a plain program's by a relative error of at most 0.007.
Values may be sent and summed in bfloat16 or wider, within the bound.
No kernel may reach another device: no remote copies, remote signals or barrier semaphores. Data moves between devices by JAX's collectives and lax.ppermute only.
A program may use at most 64 MiB of HBM per device.

v0:
```python
import jax
import jax.numpy as jnp
from jax import lax
from jax.sharding import PartitionSpec as P

LN_EPS = 1e-05
RMS_EPS = 1e-06


def shifted(value, axis, by):
    size = lax.axis_size(axis)
    pairs = [(i, i + by) for i in range(size) if 0 <= i + by < size]
    return lax.ppermute(value, axis, pairs)


def sent_to_all(value, axis):
    copies = jnp.broadcast_to(value, (lax.axis_size(axis), *value.shape))
    return lax.all_to_all(copies, axis, split_axis=0, concat_axis=0, tiled=True)


def of_everyone(value, axis):
    return sent_to_all(value, axis).sum(axis=0)


def together(arrays, axis):
    line, at, outs = (jnp.concatenate([a.reshape(-1) for a in arrays]), 0, [])
    so_far = of_everyone(line, axis)
    for a in arrays:
        outs.append(so_far[at : at + a.size].reshape(a.shape))
        at += a.size
    return tuple(outs)


def cut_along(value, dim, size):
    before, after = (value.shape[:dim], value.shape[dim + 1 :])
    return jnp.moveaxis(value.reshape(*before, size, -1, *after), dim, 0)


def summed_on_arrival(value, axis, dim):
    parts = cut_along(value, dim, lax.axis_size(axis))
    arrived = lax.all_to_all(parts, axis, split_axis=0, concat_axis=0, tiled=True)
    return arrived.sum(axis=0)


def laid_out(parts, dim):
    lengths = list(parts.shape[1:])
    lengths[dim] *= parts.shape[0]
    return jnp.moveaxis(parts, 0, dim).reshape(lengths)


def gather_directly(value, axis, dim):
    return laid_out(sent_to_all(value, axis), dim)


def body(
    resid,
    a_val,
    a_gate,
    conv_kernel,
    conv_bias,
    ln_gain,
    ln_bias,
    w_out,
    ffn_gain,
    routes,
    route_weights,
    exp_gate,
    exp_up,
    exp_down,
    sh_gate,
    sh_up,
    sh_down,
):
    tp_count = lax.axis_size("tp")
    tp_place = lax.axis_index("tp")
    sp_count = lax.axis_size("sp")
    tok_rows = resid.shape[0]
    model_width = resid.shape[1]
    col_width = model_width // tp_count
    col_start = tp_place * col_width
    conv_span = conv_kernel.shape[0]
    channels_all = a_val.shape[1] * tp_count
    gated_in = (a_val.astype(jnp.float32) * jax.nn.sigmoid(a_gate.astype(jnp.float32))).astype(
        jnp.bfloat16
    )
    before = shifted(gated_in[tok_rows - (conv_span - 1) :], "sp", 1)
    padded = jnp.concatenate([before, gated_in], axis=0).astype(jnp.float32)
    kernel = conv_kernel.astype(jnp.float32)

    def add_tap(offset, running):
        window_rows = lax.dynamic_slice_in_dim(padded, offset, tok_rows, 0)
        return running + lax.dynamic_slice_in_dim(kernel, offset, 1, 0) * window_rows

    start_sum = jnp.broadcast_to(conv_bias[None, :], gated_in.shape)
    conv_out = lax.fori_loop(0, conv_span, add_tap, start_sum)
    row_sums = together((jnp.sum(conv_out, axis=1), jnp.sum(conv_out * conv_out, axis=1)), "tp")
    channel_mean = row_sums[0] / channels_all
    channel_var = row_sums[1] / channels_all - channel_mean * channel_mean
    scaled = (conv_out - channel_mean[:, None]) * lax.rsqrt(
        channel_var[:, None] + LN_EPS
    ) * ln_gain[None, :] + ln_bias[None, :]
    mixed_out = jax.nn.silu(scaled).astype(jnp.bfloat16)
    partial_proj = jnp.dot(mixed_out, w_out, preferred_element_type=jnp.float32)
    projected = summed_on_arrival(partial_proj, "tp", 1)
    resid_cols = lax.dynamic_slice_in_dim(resid, col_start, col_width, 1)
    middle_cols = (resid_cols.astype(jnp.float32) + projected).astype(jnp.bfloat16)
    share_f = middle_cols.astype(jnp.float32)
    squares = of_everyone(jnp.sum(share_f * share_f, axis=1), "tp")
    gain_cols = lax.dynamic_slice_in_dim(ffn_gain, col_start, col_width, 0)
    inverse = lax.rsqrt(squares[:, None] / model_width + RMS_EPS)
    normed_cols = (share_f * inverse * gain_cols[None, :]).astype(jnp.bfloat16)
    normed = gather_directly(normed_cols, "tp", 1)
    shared_gate = jnp.dot(normed, sh_gate, preferred_element_type=jnp.float32)
    shared_up = jnp.dot(normed, sh_up, preferred_element_type=jnp.float32)
    shared_hidden = (jax.nn.silu(shared_gate) * shared_up).astype(jnp.bfloat16)
    weight_rows = sh_down
    shared = jnp.dot(
        lax.all_gather(shared_hidden, "tp", axis=1, tiled=True),
        weight_rows,
        preferred_element_type=jnp.float32,
    )
    top_count = routes.shape[1]
    local_experts = exp_gate.shape[0]
    experts_all = local_experts * sp_count
    capacity = max(2 * tok_rows * top_count // experts_all, tp_count)
    pair_count = tok_rows * top_count
    chosen = routes.reshape(pair_count)
    one_hot = (chosen[:, None] == jnp.arange(experts_all, dtype=jnp.int32)[None, :]).astype(
        jnp.int32
    )
    earlier = jnp.cumsum(one_hot, axis=0) - one_hot
    place_in = jnp.sum(earlier * one_hot, axis=1)
    slot_of = chosen * capacity + place_in
    owner_ids = (
        jnp.zeros((experts_all * capacity,), jnp.int32)
        .at[slot_of]
        .set(jnp.arange(pair_count, dtype=jnp.int32) + 1)
    )
    owner_grid = owner_ids.reshape(sp_count, local_experts, capacity)
    part_slots = capacity // tp_count
    own_owners = lax.dynamic_slice_in_dim(owner_grid, tp_place * part_slots, part_slots, 2)
    source_row = jnp.maximum(own_owners - 1, 0) // top_count
    taken = normed[source_row.reshape(-1)].reshape(own_owners.shape + (model_width,))
    landed = lax.all_to_all(
        jnp.where((own_owners > 0)[..., None], taken, jnp.zeros((), jnp.bfloat16)),
        "sp",
        split_axis=0,
        concat_axis=0,
        tiled=True,
    )
    arrived = lax.all_gather(landed, "tp", axis=2, tiled=True)
    gate_part = jnp.einsum("sxcd,xdf->sxcf", arrived, exp_gate, preferred_element_type=jnp.float32)
    up_part = jnp.einsum("sxcd,xdf->sxcf", arrived, exp_up, preferred_element_type=jnp.float32)
    expert_hidden = (jax.nn.silu(gate_part) * up_part).astype(jnp.bfloat16)
    weight_rows = exp_down
    expert_sum = jnp.einsum(
        "sxcf,xfd->sxcd",
        lax.all_gather(expert_hidden, "tp", axis=3, tiled=True),
        weight_rows,
        preferred_element_type=jnp.float32,
    )
    expert_out = expert_sum.astype(jnp.bfloat16)
    returned = lax.all_to_all(expert_out, "sp", split_axis=0, concat_axis=0, tiled=True)
    flat_out = returned.reshape(experts_all * capacity, col_width)
    picked = flat_out[slot_of].astype(jnp.float32).reshape(tok_rows, top_count, col_width)
    routed = jnp.sum(picked * route_weights[:, :, None], axis=1)
    return (middle_cols.astype(jnp.float32) + shared + routed).astype(jnp.bfloat16)


def solution(mesh):
    in_specs = (
        P("sp", None),
        P("sp", "tp"),
        P("sp", "tp"),
        P(None, "tp"),
        P("tp"),
        P("tp"),
        P("tp"),
        P("tp", None),
        P(),
        P("sp", None),
        P("sp", None),
        P("sp", None, "tp"),
        P("sp", None, "tp"),
        P("sp", None, "tp"),
        P(None, "tp"),
        P(None, "tp"),
        P(None, "tp"),
    )
    out_specs = P("sp", "tp")
    return jax.shard_map(body, mesh=mesh, in_specs=in_specs, out_specs=out_specs, check_vma=False)
```

profile of v0, /device:TPU:1, one launch (start us, length us, event | category | flops | bytes accessed | tf_op | source)
XLA Modules:
  0.0 289.1 jit_solution(5192437029576323760)
XLA Ops:
  6.5 0.9 multiply_convert_fusion.1
  7.5 3.9 %collective-permute-start = (bf16[30,64]{0,1:T(8,128)(2,1)S(1)}, bf16[30,64]{0,1:T(8,128)(2,1)S(1)}, u32[]{:S(2)}, u32[]{:S(2)}) collective-permute-start(bf16[30,64]{0,1:T(8,128)(2,1)S(1)} %slice.24), channel_id=1, source_target_pairs={{0,16},{16,32},{32,48},{48,64},{64,80},{80,96},{96,112},{112,128},... | collective-permute-start | bytes 11528 | tf_op jit(solution)/shard_map/ppermute | solution.py:13
  11.4 0.7 convert_element_type.67
  12.1 0.1 collective-permute-done
  12.3 0.7 broadcast_in_dim.20
  13.0 7.4 %while.13 = (s32[]{:T(128)}, f32[128,64]{1,0:T(8,128)S(1)}, f32[31,64]{1,0:T(8,128)S(1)}, f32[158,64]{0,1:T(8,128)S(1)}, s32[]{:T(128)}) while((s32[]{:T(128)}, f32[128,64]{1,0:T(8,128)S(1)}, f32[31,64]{1,0:T(8,128)S(1)}, f32[158,64]{0,1:T(8,128)S(1)}, s32[]{:T(128)}) %tuple.33), condition=%wide.region_1.0_spmd, body=%wide.region_0.0_spmd.sunk | while | flops 16386 | bytes 230221 | solution.py:95
  20.5 0.6 broadcast_in_dim.21
  21.2 8.6 %all-to-all-start = ((f32[16,1,256]{2,1,0:T(1,128)}), f32[16,1,256]{2,1,0:T(1,128)S(1)}, u32[]{:S(2)}, u32[]{:S(2)}) async-start(f32[16,1,256]{2,1,0:T(1,128)} %broadcast_in_dim.21), calls=%async_computation | async-start | bytes 32768 | tf_op jit(solution)/shard_map/all_to_all | solution.py:18
  29.9 7.3 %all-to-all-done = f32[16,1,256]{2,1,0:T(1,128)S(1)} async-done(((f32[16,1,256]{2,1,0:T(1,128)}), f32[16,1,256]{2,1,0:T(1,128)S(1)}, u32[]{:S(2)}, u32[]{:S(2)}) %all-to-all-start) | async-done | bytes 16416 | tf_op jit(solution)/shard_map/all_to_all | solution.py:18
  37.2 1.4 convolution_bitcast_fusion
  38.6 1.1 copy.143
  39.7 3.8 %all-to-all-start.1 = ((f32[16,128,128]{2,1,0:T(8,128)}), f32[16,128,128]{2,1,0:T(8,128)S(1)}, u32[]{:S(2)}, u32[]{:S(2)}) async-start(f32[16,128,128]{2,1,0:T(8,128)} %bitcast.117), calls=%async_computation.1 | async-start | bytes 2097152 | tf_op jit(solution)/shard_map/all_to_all | solution.py:41
  43.5 0.1 copy.103
  43.8 0.1 eq.25
  43.9 0.1 copy.102
  44.1 1.2 reduce-window.6
  45.3 0.2 slice_reduce_fusion
  45.6 0.1 fusion.39
  45.7 25.9 %all-to-all-done.1 = f32[16,128,128]{2,1,0:T(8,128)S(1)} async-done(((f32[16,128,128]{2,1,0:T(8,128)}), f32[16,128,128]{2,1,0:T(8,128)S(1)}, u32[]{:S(2)}, u32[]{:S(2)}) %all-to-all-start.1) | async-done | bytes 1048608 | tf_op jit(solution)/shard_map/all_to_all | solution.py:41
  71.6 0.9 fusion.34
  72.5 0.6 broadcast_in_dim.26
  73.1 3.4 %all-to-all-start.2 = ((f32[16,1,128]{2,1,0:T(1,128)}), f32[16,1,128]{2,1,0:T(1,128)S(1)}, u32[]{:S(2)}, u32[]{:S(2)}) async-start(f32[16,1,128]{2,1,0:T(1,128)} %broadcast_in_dim.26), calls=%async_computation.2 | async-start | bytes 16384 | tf_op jit(solution)/shard_map/all_to_all | solution.py:18
  76.6 0.8 dynamic_slice.24
  77.3 6.2 %all-to-all-done.2 = f32[16,1,128]{2,1,0:T(1,128)S(1)} async-done(((f32[16,1,128]{2,1,0:T(1,128)}), f32[16,1,128]{2,1,0:T(1,128)S(1)}, u32[]{:S(2)}, u32[]{:S(2)}) %all-to-all-start.2) | async-done | bytes 8224 | tf_op jit(solution)/shard_map/all_to_all | solution.py:18
  83.7 0.9 broadcast_in_dim.27
  84.6 4.0 %all-to-all-start.3 = ((bf16[16,128,128]{2,1,0:T(8,128)(2,1)}), bf16[16,128,128]{2,1,0:T(8,128)(2,1)S(1)}, u32[]{:S(2)}, u32[]{:S(2)}) async-start(bf16[16,128,128]{2,1,0:T(8,128)(2,1)} %broadcast_in_dim.27), calls=%async_computation.3 | async-start | bytes 1048576 | tf_op jit(solution)/shard_map/all_to_all | solution.py:18
  88.6 2.4 scatter_custom_fusion
  91.3 0.1 copy.107
  91.7 14.2 %all-to-all-done.3 = bf16[16,128,128]{2,1,0:T(8,128)(2,1)S(1)} async-done(((bf16[16,128,128]{2,1,0:T(8,128)(2,1)}), bf16[16,128,128]{2,1,0:T(8,128)(2,1)S(1)}, u32[]{:S(2)}, u32[]{:S(2)}) %all-to-all-start.3) | async-done | bytes 524320 | tf_op jit(solution)/shard_map/all_to_all | solution.py:18
  106.0 0.7 gather_fusion
  106.7 0.2 reshape.161
  106.9 0.3 broadcast_select_fusion
  107.2 27.0 %all_to_all.32 = bf16[32,1,2,2048]{3,2,1,0:T(2,128)(2,1)S(1)} all-to-all(bf16[32,1,2,2048]{3,2,1,0:T(2,128)(2,1)S(1)} %broadcast_select_fusion), channel_id=1, replica_groups=mesh['sp'=32,'tp'=16] {'sp'}, dimensions={0} | all-to-all | bytes 524288 | tf_op jit(solution)/shard_map/all_to_all | solution.py:144
  134.2 0.8 copy.110
  135.0 0.2 all-gather.5.cloned.1.call-start
  135.2 35.9 %all-gather.3.cloned.1.call-done = bf16[32,1,32,2048]{3,0,1,2:T(8,128)(2,1)} async-done(((bf16[32,1,2,2048]{3,0,1,2:T(8,128)(2,1)}), bf16[32,1,32,2048]{3,0,1,2:T(8,128)(2,1)}) %all-gather.3.cloned.1.call-update) | async-done | bytes 4194320 | tf_op jit(solution)/shard_map/all_gather | solution.py:151
  171.2 5.2 %fusion.9 = f32[32,1,32,256]{3,2,0,1:T(8,128)S(1)} fusion(bf16[32,1,32,2048]{3,0,1,2:T(8,128)(2,1)} %all-gather.3.cloned.1.call-done, bf16[1,2048,256]{2,1,0:T(8,128)(2,1)S(1)} %copy-done), kind=kOutput, calls=%fused_computation.15 | convolution fusion | flops 1073741824 | bytes 6291456 | tf_op jit(solution)/shard_map/sxcd,xdf->sxcf/dot_general | solution.py:152
  176.4 3.8 %fusion.18 = bf16[32,1,32,256]{3,2,0,1:T(8,128)(2,1)} fusion(bf16[32,1,32,2048]{3,0,1,2:T(8,128)(2,1)S(1)} %copy-done.4, bf16[1,2048,256]{2,1,0:T(8,128)(2,1)S(1)} %copy-done.5, f32[32,1,32,256]{3,2,0,1:T(8,128)S(1)} %fusion.9), kind=kOutput, calls=%fused_computation.19 | convolution fusion | flops 1075314688 | bytes 6815744 | tf_op jit(solution)/shard_map/sxcd,xdf->sxcf/dot_general | solution.py:153
  180.2 0.1 copy.113
  180.4 68.2 %all-gather.5.cloned.1.call-done = bf16[32,1,32,4096]{3,2,0,1:T(8,128)(2,1)} async-done(((bf16[32,1,32,256]{3,2,0,1:T(8,128)(2,1)}), bf16[32,1,32,4096]{3,2,0,1:T(8,128)(2,1)}) %all-gather.5.cloned.1.call-update) | async-done | bytes 8388624 | tf_op jit(solution)/shard_map/all_gather | solution.py:158
  248.6 6.6 %fusion.24 = bf16[32,1,32,128]{3,2,1,0:T(8,128)(2,1)} fusion(bf16[32,1,32,4096]{3,2,0,1:T(8,128)(2,1)} %all-gather.5.cloned.1.call-done, bf16[1,4096,128]{2,1,0:T(8,128)(2,1)} %param.32), kind=kOutput, calls=%fused_computation.21 | convolution fusion | flops 1073872896 | bytes 9699328 | tf_op jit(solution)/shard_map/sxcf,xfd->sxcd/dot_general | solution.py:156
  255.2 6.9 %all-to-all-start.5 = ((bf16[32,1,32,128]{3,2,1,0:T(8,128)(2,1)}), bf16[32,1,32,128]{3,2,1,0:T(8,128)(2,1)S(1)}, u32[]{:S(2)}, u32[]{:S(2)}) async-start(bf16[32,1,32,128]{3,2,1,0:T(8,128)(2,1)} %fusion.24), calls=%async_computation.5 | async-start | bytes 524288 | tf_op jit(solution)/shard_map/all_to_all | solution.py:163
  262.1 0.3 fusion.50
  262.4 0.3 fusion.29
  262.7 17.1 %all_gather.9 = bf16[128,512]{0,1:T(8,128)(2,1)S(1)} all-gather(bf16[128,32]{0,1:T(8,128)(2,1)S(1)} %fusion.29), channel_id=1, replica_groups=mesh['sp'=32,'tp'=16] {'tp'}, dimensions={1}, use_global_device_ids=true | all-gather | bytes 139264 | tf_op jit(solution)/shard_map/all_gather | solution.py:118
  279.8 1.3 gather_fusion.1
  281.2 0.2 fusion.33
  281.4 0.9 fusion.28
  (174 shorter events, 7.8 us)
Async XLA Ops:
  6.5 164.6 %copy-start = (bf16[1,2048,256]{2,1,0:T(8,128)(2,1)S(1)}, bf16[1,2048,256]{2,1,0:T(8,128)(2,1)}, u32[]{:S(2)}) copy-start(bf16[1,2048,256]{2,1,0:T(8,128)(2,1)} %param.30) | copy-start | bytes 3145732
  6.5 37.0 %copy-start.2 = (s32[128,4]{0,1:T(4,128)S(1)}, s32[128,4]{0,1:T(4,128)}, u32[]{:S(2)}) copy-start(s32[128,4]{0,1:T(4,128)} %param.28) | copy-start | bytes 6148
  7.5 4.8 %collective-permute-start = (bf16[30,64]{0,1:T(8,128)(2,1)S(1)}, bf16[30,64]{0,1:T(8,128)(2,1)S(1)}, u32[]{:S(2)}, u32[]{:S(2)}) collective-permute-start(bf16[30,64]{0,1:T(8,128)(2,1)S(1)} %slice.24), channel_id=1, source_target_pairs={{0,16},{16,32},{32,48},{48,64},{64,80},{80,96},{96,112},{112,128},... | collective-permute-start | bytes 11528 | tf_op jit(solution)/shard_map/ppermute | solution.py:13
  21.2 16.0 %all-to-all-start = ((f32[16,1,256]{2,1,0:T(1,128)}), f32[16,1,256]{2,1,0:T(1,128)S(1)}, u32[]{:S(2)}, u32[]{:S(2)}) async-start(f32[16,1,256]{2,1,0:T(1,128)} %broadcast_in_dim.21), calls=%async_computation | async-start | bytes 32768 | tf_op jit(solution)/shard_map/all_to_all | solution.py:18
  39.7 31.9 %all-to-all-start.1 = ((f32[16,128,128]{2,1,0:T(8,128)}), f32[16,128,128]{2,1,0:T(8,128)S(1)}, u32[]{:S(2)}, u32[]{:S(2)}) async-start(f32[16,128,128]{2,1,0:T(8,128)} %bitcast.117), calls=%async_computation.1 | async-start | bytes 2097152 | tf_op jit(solution)/shard_map/all_to_all | solution.py:41
  73.1 10.4 %all-to-all-start.2 = ((f32[16,1,128]{2,1,0:T(1,128)}), f32[16,1,128]{2,1,0:T(1,128)S(1)}, u32[]{:S(2)}, u32[]{:S(2)}) async-start(f32[16,1,128]{2,1,0:T(1,128)} %broadcast_in_dim.26), calls=%async_computation.2 | async-start | bytes 16384 | tf_op jit(solution)/shard_map/all_to_all | solution.py:18
  84.6 21.3 %all-to-all-start.3 = ((bf16[16,128,128]{2,1,0:T(8,128)(2,1)}), bf16[16,128,128]{2,1,0:T(8,128)(2,1)S(1)}, u32[]{:S(2)}, u32[]{:S(2)}) async-start(bf16[16,128,128]{2,1,0:T(8,128)(2,1)} %broadcast_in_dim.27), calls=%async_computation.3 | async-start | bytes 1048576 | tf_op jit(solution)/shard_map/all_to_all | solution.py:18
  88.6 82.6 %all-gather.3.cloned.1.call-start = ((), (), s32[]{:S(2)}) async-start(), calls=%async_computation.6 | async-start | bytes 4456448 | tf_op jit(solution)/shard_map/all_gather | solution.py:151
  135.0 41.4 %copy-start.5 = (bf16[1,2048,256]{2,1,0:T(8,128)(2,1)S(1)}, bf16[1,2048,256]{2,1,0:T(8,128)(2,1)}, u32[]{:S(2)}) copy-start(bf16[1,2048,256]{2,1,0:T(8,128)(2,1)} %param.31) | copy-start | bytes 3145732
  135.0 113.6 %all-gather.5.cloned.1.call-start = ((), (), s32[]{:S(2)}) async-start(), calls=%async_computation.7 | async-start | bytes 8912896 | tf_op jit(solution)/shard_map/all_gather | solution.py:158
  171.2 5.2 %copy-start.4 = (bf16[32,1,32,2048]{3,0,1,2:T(8,128)(2,1)S(1)}, bf16[32,1,32,2048]{3,0,1,2:T(8,128)(2,1)}, u32[]{:S(2)}) copy-start(bf16[32,1,32,2048]{3,0,1,2:T(8,128)(2,1)} %all-gather.3.cloned.1.call-done) | copy-start | bytes 12582916
  176.4 3.8 %copy-start.3 = (f32[128,4]{0,1:T(4,128)S(1)}, f32[128,4]{0,1:T(4,128)}, u32[]{:S(2)}) copy-start(f32[128,4]{0,1:T(4,128)} %param.29) | copy-start | bytes 6148
  180.4 81.8 %copy-start.6 = (bf16[2048,32]{0,1:T(8,128)(2,1)S(1)}, bf16[2048,32]{0,1:T(8,128)(2,1)}, u32[]{:S(2)}) copy-start(bf16[2048,32]{0,1:T(8,128)(2,1)} %param.33) | copy-start | bytes 393220
  180.4 82.0 %copy-start.7 = (bf16[2048,32]{0,1:T(8,128)(2,1)S(1)}, bf16[2048,32]{0,1:T(8,128)(2,1)}, u32[]{:S(2)}) copy-start(bf16[2048,32]{0,1:T(8,128)(2,1)} %param.34) | copy-start | bytes 393220
  180.4 101.0 %copy-start.1 = (bf16[512,128]{1,0:T(8,128)(2,1)S(1)}, bf16[512,128]{1,0:T(8,128)(2,1)}, u32[]{:S(2)}) copy-start(bf16[512,128]{1,0:T(8,128)(2,1)} %param.35) | copy-start | bytes 393220
  255.2 24.6 %all-to-all-start.5 = ((bf16[32,1,32,128]{3,2,1,0:T(8,128)(2,1)}), bf16[32,1,32,128]{3,2,1,0:T(8,128)(2,1)S(1)}, u32[]{:S(2)}, u32[]{:S(2)}) async-start(bf16[32,1,32,128]{3,2,1,0:T(8,128)(2,1)} %fusion.24), calls=%async_computation.5 | async-start | bytes 524288 | tf_op jit(solution)/shard_map/all_to_all | solution.py:163
Sparse Core Ops, SparseCore 0:
  135.1 36.0 all-gather.2
  180.3 68.1 all-gather.4
where the time goes:
time: 290 us; the launch traced here: 289 us
  waiting for transfers between devices  158 us (54%)
  blocking collectives  44.1 us (15%)
  starting transfers between devices  31 us (11%)
  matrix products  18.4 us (6%)
  local copies, waits for them, and re-layouts  17.6 us (6%)
  between operations  13.7 us (5%)
  other arithmetic  5.28 us (2%)
    all_gather x1, waiting for transfers between devices, body(): lax.all_gather(expert_hidden, 'tp', axis=3, tiled=True)  68.2 us
    all_gather x1, waiting for transfers between devices, body(): arrived = lax.all_gather(landed, 'tp', axis=2, tiled=True)  35.9 us
    all_to_all x3, waiting for transfers between devices, sent_to_all(): return lax.all_to_all(copies, axis, split_axis=0, concat_axis=0, tiled=True)  27.7 us
    all_to_all x1, blocking collectives, body(): lax.all_to_all(jnp.where((own_owners > 0)[..., None], taken, jnp.zeros(()...  27 us
    all_to_all x1, waiting for transfers between devices, summed_on_arrival(): lax.all_to_all(parts, axis, split_axis=0, concat_axis=0, tiled=True)  25.9 us
    all_gather x1, blocking collectives, body(): lax.all_gather(shared_hidden, 'tp', axis=1, tiled=True)  17.1 us
    all_to_all x3, starting transfers between devices, sent_to_all(): return lax.all_to_all(copies, axis, split_axis=0, concat_axis=0, tiled=True)  16.1 us
    all_to_all x1, starting transfers between devices, body(): lax.all_to_all(expert_out, 'sp', split_axis=0, concat_axis=0, tiled=True)  6.89 us
  transfers between devices with their start and end apart: 8, of which 7 were waited for; matrix products, arithmetic and copies ran while one was open for 3% of the time, Pallas kernels for 0%

commit v1 on v0

--- a/solution.py
+++ b/solution.py
@@ -148,7 +148,10 @@
         concat_axis=0,
         tiled=True,
     )
-    arrived = lax.all_gather(landed, "tp", axis=2, tiled=True)
+    count = lax.axis_size("tp")
+    tiles = jnp.stack([landed for _ in range(count)])
+    tiles = lax.all_to_all(tiles, "tp", split_axis=0, concat_axis=0)
+    arrived = jnp.concatenate(tiles, axis=2)
     gate_part = jnp.einsum("sxcd,xdf->sxcf", arrived, exp_gate, preferred_element_type=jnp.float32)
     up_part = jnp.einsum("sxcd,xdf->sxcf", arrived, exp_up, preferred_element_type=jnp.float32)
     expert_hidden = (jax.nn.silu(gate_part) * up_part).astype(jnp.bfloat16)

time: 290 us -> 358 us (1.23)
  blocking collectives: 44.1 us -> 143 us
  waiting for transfers between devices: 158 us -> 114 us
  local copies, waits for them, and re-layouts: 17.6 us -> 33.8 us
    all_to_all x0 -> x1, blocking collectives: none -> 99.3 us  [body(): tiles = lax.all_to_all(tiles, 'tp', split_axis=0, concat_axis=0)]
    all_gather x1 -> x0, waiting for transfers between devices: 35.9 us -> none  [body(): arrived = lax.all_gather(landed, 'tp', axis=2, tiled=True)]
    another operation x1 -> x3, local copies, waits for them, and re-layouts: 0.01 us -> 10.4 us
    all_gather x1, waiting for transfers between devices: 68.2 us -> 60.4 us  [body(): lax.all_gather(expert_hidden, 'tp', axis=3, tiled=True)]
    reshape x0 -> x1, local copies, waits for them, and re-layouts: none -> 6.47 us  [body(): arrived = jnp.concatenate(tiles, axis=2)]
  transfers between devices with their start and end apart: 8 -> 7, of which waited for: 7 -> 6; matrix products, arithmetic and copies ran while one was open for 3% -> 2% of each run, Pallas kernels for 0% -> 0%
where the time goes in v1:
time: 358 us; the launch traced here: 357 us
  blocking collectives  143 us (40%)
  waiting for transfers between devices  114 us (32%)
  local copies, waits for them, and re-layouts  33.8 us (9%)
  starting transfers between devices  30.7 us (9%)
  matrix products  15.2 us (4%)
  between operations  13.7 us (4%)
  other arithmetic  5.21 us (1%)
    all_to_all x1, blocking collectives, body(): tiles = lax.all_to_all(tiles, 'tp', split_axis=0, concat_axis=0)  99.3 us
    all_gather x1, waiting for transfers between devices, body(): lax.all_gather(expert_hidden, 'tp', axis=3, tiled=True)  60.4 us
    all_to_all x3, waiting for transfers between devices, sent_to_all(): return lax.all_to_all(copies, axis, split_axis=0, concat_axis=0, tiled=True)  27.7 us
    all_to_all x1, blocking collectives, body(): lax.all_to_all(jnp.where((own_owners > 0)[..., None], taken, jnp.zeros(()...  27 us
    all_to_all x1, waiting for transfers between devices, summed_on_arrival(): lax.all_to_all(parts, axis, split_axis=0, concat_axis=0, tiled=True)  25.9 us
    all_gather x1, blocking collectives, body(): lax.all_gather(shared_hidden, 'tp', axis=1, tiled=True)  17.1 us
    all_to_all x3, starting transfers between devices, sent_to_all(): return lax.all_to_all(copies, axis, split_axis=0, concat_axis=0, tiled=True)  16.1 us
    another operation x2, local copies, waits for them, and re-layouts  7.21 us
  transfers between devices with their start and end apart: 7, of which 6 were waited for; matrix products, arithmetic and copies ran while one was open for 2% of the time, Pallas kernels for 0%

profile of v1, /device:TPU:1, one launch (start us, length us, event | category | flops | bytes accessed | tf_op | source)
XLA Modules:
  0.0 357.4 jit_solution(8396114626639374666)
XLA Ops:
  6.5 0.9 multiply_convert_fusion.1
  7.5 3.9 %collective-permute-start = (bf16[30,64]{0,1:T(8,128)(2,1)S(1)}, bf16[30,64]{0,1:T(8,128)(2,1)S(1)}, u32[]{:S(2)}, u32[]{:S(2)}) collective-permute-start(bf16[30,64]{0,1:T(8,128)(2,1)S(1)} %slice.24), channel_id=1, source_target_pairs={{0,16},{16,32},{32,48},{48,64},{64,80},{80,96},{96,112},{112,128},... | collective-permute-start | bytes 11528 | tf_op jit(solution)/shard_map/ppermute | solution.py:13
  11.4 0.7 convert_element_type.67
  12.1 0.1 collective-permute-done
  12.3 0.7 broadcast_in_dim.20
  13.0 7.4 %while.13 = (s32[]{:T(128)}, f32[128,64]{1,0:T(8,128)S(1)}, f32[31,64]{1,0:T(8,128)S(1)}, f32[158,64]{0,1:T(8,128)S(1)}, s32[]{:T(128)}) while((s32[]{:T(128)}, f32[128,64]{1,0:T(8,128)S(1)}, f32[31,64]{1,0:T(8,128)S(1)}, f32[158,64]{0,1:T(8,128)S(1)}, s32[]{:T(128)}) %tuple.33), condition=%wide.region_1.0_spmd, body=%wide.region_0.0_spmd.sunk | while | flops 16386 | bytes 230221 | solution.py:95
  20.5 0.6 broadcast_in_dim.21
  21.1 8.6 %all-to-all-start = ((f32[16,1,256]{2,1,0:T(1,128)}), f32[16,1,256]{2,1,0:T(1,128)S(1)}, u32[]{:S(2)}, u32[]{:S(2)}) async-start(f32[16,1,256]{2,1,0:T(1,128)} %broadcast_in_dim.21), calls=%async_computation | async-start | bytes 32768 | tf_op jit(solution)/shard_map/all_to_all | solution.py:18
  29.8 7.3 %all-to-all-done = f32[16,1,256]{2,1,0:T(1,128)S(1)} async-done(((f32[16,1,256]{2,1,0:T(1,128)}), f32[16,1,256]{2,1,0:T(1,128)S(1)}, u32[]{:S(2)}, u32[]{:S(2)}) %all-to-all-start) | async-done | bytes 16416 | tf_op jit(solution)/shard_map/all_to_all | solution.py:18
  37.1 1.4 convolution_bitcast_fusion.2
  38.5 1.1 copy.122
  39.6 3.8 %all-to-all-start.1 = ((f32[16,128,128]{2,1,0:T(8,128)}), f32[16,128,128]{2,1,0:T(8,128)S(1)}, u32[]{:S(2)}, u32[]{:S(2)}) async-start(f32[16,128,128]{2,1,0:T(8,128)} %bitcast.110), calls=%async_computation.1 | async-start | bytes 2097152 | tf_op jit(solution)/shard_map/all_to_all | solution.py:41
  43.5 0.1 copy.99
  43.8 0.1 copy.98
  44.1 1.2 reduce-window.6
  45.2 0.2 slice_reduce_fusion
  45.5 0.1 fusion.23
  45.6 25.9 %all-to-all-done.1 = f32[16,128,128]{2,1,0:T(8,128)S(1)} async-done(((f32[16,128,128]{2,1,0:T(8,128)}), f32[16,128,128]{2,1,0:T(8,128)S(1)}, u32[]{:S(2)}, u32[]{:S(2)}) %all-to-all-start.1) | async-done | bytes 1048608 | tf_op jit(solution)/shard_map/all_to_all | solution.py:41
  71.6 0.9 fusion.18
  72.4 0.6 broadcast_in_dim.26
  73.1 3.4 all-to-all-start.2
  76.5 0.8 dynamic_slice.24
  77.3 6.2 %all-to-all-done.2 = f32[16,1,128]{2,1,0:T(1,128)S(1)} async-done(((f32[16,1,128]{2,1,0:T(1,128)}), f32[16,1,128]{2,1,0:T(1,128)S(1)}, u32[]{:S(2)}, u32[]{:S(2)}) %all-to-all-start.2) | async-done | bytes 8224 | tf_op jit(solution)/shard_map/all_to_all | solution.py:18
  83.6 0.9 broadcast_in_dim.27
  84.5 4.0 %all-to-all-start.3 = ((bf16[16,128,128]{2,1,0:T(8,128)(2,1)}), bf16[16,128,128]{2,1,0:T(8,128)(2,1)S(1)}, u32[]{:S(2)}, u32[]{:S(2)}) async-start(bf16[16,128,128]{2,1,0:T(8,128)(2,1)} %broadcast_in_dim.27), calls=%async_computation.3 | async-start | bytes 1048576 | tf_op jit(solution)/shard_map/all_to_all | solution.py:18
  88.5 2.4 scatter_custom_fusion
  91.6 14.2 %all-to-all-done.3 = bf16[16,128,128]{2,1,0:T(8,128)(2,1)S(1)} async-done(((bf16[16,128,128]{2,1,0:T(8,128)(2,1)}), bf16[16,128,128]{2,1,0:T(8,128)(2,1)S(1)}, u32[]{:S(2)}, u32[]{:S(2)}) %all-to-all-start.3) | async-done | bytes 524320 | tf_op jit(solution)/shard_map/all_to_all | solution.py:18
  105.9 0.7 gather_fusion
  106.6 0.2 reshape.170
  106.8 0.3 broadcast_select_fusion
  107.1 27.0 %all_to_all.40 = bf16[32,1,2,2048]{3,2,1,0:T(2,128)(2,1)S(1)} all-to-all(bf16[32,1,2,2048]{3,2,1,0:T(2,128)(2,1)S(1)} %broadcast_select_fusion), channel_id=1, replica_groups=mesh['sp'=32,'tp'=16] {'sp'}, dimensions={0} | all-to-all | bytes 524288 | tf_op jit(solution)/shard_map/all_to_all | solution.py:144
  134.1 3.2 stack.2
  137.4 99.3 %all_to_all.41 = bf16[16,32,1,2,2048]{4,3,1,2,0:T(2,128)(2,1)S(1)} all-to-all(bf16[16,32,1,2,2048]{4,3,1,2,0:T(2,128)(2,1)S(1)} %stack.2), channel_id=1, replica_groups=mesh['sp'=32,'tp'=16] {'tp'}, dimensions={0} | all-to-all | bytes 8388608 | tf_op jit(solution)/shard_map/all_to_all | solution.py:153
  236.7 6.5 %copy.106 = bf16[32,1,16,2,2048]{4,3,2,0,1:T(2,128)(2,1)} copy(bf16[32,1,16,2,2048]{4,3,0,1,2:T(2,128)(2,1)S(1)} %bitcast.114) | data formatting | bytes 8388608 | tf_op jit(solution)/shard_map/reshape | solution.py:154
  243.2 7.2 %reshape.172 = bf16[32,32,2048]{2,1,0:T(8,128)(2,1)} reshape(bf16[32,1,16,2,2048]{4,3,2,0,1:T(2,128)(2,1)} %copy.106) | data formatting | bytes 8388608 | tf_op jit(solution)/shard_map/reshape.6
  250.4 3.6 %convolution_bitcast_fusion.1 = f32[32,1,32,256]{3,2,0,1:T(8,128)S(1)} fusion(bf16[32,32,2048]{2,1,0:T(8,128)(2,1)} %reshape.172, bf16[1,2048,256]{2,1,0:T(8,128)(2,1)S(1)} %copy-done), kind=kOutput, calls=%fused_computation.11 | convolution fusion | flops 1073741824 | bytes 6291456 | tf_op jit(solution)/shard_map/sxcd,xdf->sxcf/dot_general | solution.py:155
  254.0 0.1 copy-done.5
  254.2 2.1 fusion.4
  256.3 0.1 copy.108
  256.5 60.4 %all-gather.2.cloned.1.call-done = bf16[32,1,32,4096]{3,2,0,1:T(8,128)(2,1)} async-done(((bf16[32,1,32,256]{3,2,0,1:T(8,128)(2,1)}), bf16[32,1,32,4096]{3,2,0,1:T(8,128)(2,1)}) %all-gather.2.cloned.1.call-update) | async-done | bytes 8388624 | tf_op jit(solution)/shard_map/all_gather | solution.py:161
  316.9 6.6 %fusion.8 = bf16[32,1,32,128]{3,2,1,0:T(8,128)(2,1)} fusion(bf16[32,1,32,4096]{3,2,0,1:T(8,128)(2,1)} %all-gather.2.cloned.1.call-done, bf16[1,4096,128]{2,1,0:T(8,128)(2,1)} %param.32), kind=kOutput, calls=%fused_computation.15 | convolution fusion | flops 1073872896 | bytes 9699328 | tf_op jit(solution)/shard_map/sxcf,xfd->sxcd/dot_general | solution.py:159
  323.5 6.9 %all-to-all-start.6 = ((bf16[32,1,32,128]{3,2,1,0:T(8,128)(2,1)}), bf16[32,1,32,128]{3,2,1,0:T(8,128)(2,1)S(1)}, u32[]{:S(2)}, u32[]{:S(2)}) async-start(bf16[32,1,32,128]{3,2,1,0:T(8,128)(2,1)} %fusion.8), calls=%async_computation.6 | async-start | bytes 524288 | tf_op jit(solution)/shard_map/all_to_all | solution.py:166
  330.4 0.3 fusion.34
  330.7 0.3 fusion.13
  331.0 17.1 %all_gather.6 = bf16[128,512]{0,1:T(8,128)(2,1)S(1)} all-gather(bf16[128,32]{0,1:T(8,128)(2,1)S(1)} %fusion.13), channel_id=1, replica_groups=mesh['sp'=32,'tp'=16] {'tp'}, dimensions={1}, use_global_device_ids=true | all-gather | bytes 139264 | tf_op jit(solution)/shard_map/all_gather | solution.py:118
  348.1 1.3 gather_fusion.1
  349.4 0.2 fusion.17
  349.7 0.8 fusion.12
  (174 shorter events, 7.9 us)
Async XLA Ops:
  6.5 243.9 %copy-start = (bf16[1,2048,256]{2,1,0:T(8,128)(2,1)S(1)}, bf16[1,2048,256]{2,1,0:T(8,128)(2,1)}, u32[]{:S(2)}) copy-start(bf16[1,2048,256]{2,1,0:T(8,128)(2,1)} %param.30) | copy-start | bytes 3145732
  6.5 36.9 %copy-start.3 = (s32[128,4]{0,1:T(4,128)S(1)}, s32[128,4]{0,1:T(4,128)}, u32[]{:S(2)}) copy-start(s32[128,4]{0,1:T(4,128)} %param.28) | copy-start | bytes 6148
  7.5 4.8 %collective-permute-start = (bf16[30,64]{0,1:T(8,128)(2,1)S(1)}, bf16[30,64]{0,1:T(8,128)(2,1)S(1)}, u32[]{:S(2)}, u32[]{:S(2)}) collective-permute-start(bf16[30,64]{0,1:T(8,128)(2,1)S(1)} %slice.24), channel_id=1, source_target_pairs={{0,16},{16,32},{32,48},{48,64},{64,80},{80,96},{96,112},{112,128},... | collective-permute-start | bytes 11528 | tf_op jit(solution)/shard_map/ppermute | solution.py:13
  21.1 16.0 %all-to-all-start = ((f32[16,1,256]{2,1,0:T(1,128)}), f32[16,1,256]{2,1,0:T(1,128)S(1)}, u32[]{:S(2)}, u32[]{:S(2)}) async-start(f32[16,1,256]{2,1,0:T(1,128)} %broadcast_in_dim.21), calls=%async_computation | async-start | bytes 32768 | tf_op jit(solution)/shard_map/all_to_all | solution.py:18
  39.6 31.9 %all-to-all-start.1 = ((f32[16,128,128]{2,1,0:T(8,128)}), f32[16,128,128]{2,1,0:T(8,128)S(1)}, u32[]{:S(2)}, u32[]{:S(2)}) async-start(f32[16,128,128]{2,1,0:T(8,128)} %bitcast.110), calls=%async_computation.1 | async-start | bytes 2097152 | tf_op jit(solution)/shard_map/all_to_all | solution.py:41
  73.1 10.4 %all-to-all-start.2 = ((f32[16,1,128]{2,1,0:T(1,128)}), f32[16,1,128]{2,1,0:T(1,128)S(1)}, u32[]{:S(2)}, u32[]{:S(2)}) async-start(f32[16,1,128]{2,1,0:T(1,128)} %broadcast_in_dim.26), calls=%async_computation.2 | async-start | bytes 16384 | tf_op jit(solution)/shard_map/all_to_all | solution.py:18
  84.5 21.3 %all-to-all-start.3 = ((bf16[16,128,128]{2,1,0:T(8,128)(2,1)}), bf16[16,128,128]{2,1,0:T(8,128)(2,1)S(1)}, u32[]{:S(2)}, u32[]{:S(2)}) async-start(bf16[16,128,128]{2,1,0:T(8,128)(2,1)} %broadcast_in_dim.27), calls=%async_computation.3 | async-start | bytes 1048576 | tf_op jit(solution)/shard_map/all_to_all | solution.py:18
  88.5 228.4 %all-gather.2.cloned.1.call-start = ((), (), s32[]{:S(2)}) async-start(), calls=%async_computation.7 | async-start | bytes 8912896 | tf_op jit(solution)/shard_map/all_gather | solution.py:161
  250.4 3.6 %copy-start.1 = (bf16[32,32,2048]{2,1,0:T(8,128)(2,1)S(1)}, bf16[32,32,2048]{2,1,0:T(8,128)(2,1)}, u32[]{:S(2)}) copy-start(bf16[32,32,2048]{2,1,0:T(8,128)(2,1)} %reshape.172) | copy-start | bytes 12582916
  250.4 3.7 %copy-start.5 = (bf16[1,2048,256]{2,1,0:T(8,128)(2,1)S(1)}, bf16[1,2048,256]{2,1,0:T(8,128)(2,1)}, u32[]{:S(2)}) copy-start(bf16[1,2048,256]{2,1,0:T(8,128)(2,1)} %param.31) | copy-start | bytes 3145732
  254.2 2.2 copy-start.4
  256.4 74.0 %copy-start.6 = (bf16[2048,32]{0,1:T(8,128)(2,1)S(1)}, bf16[2048,32]{0,1:T(8,128)(2,1)}, u32[]{:S(2)}) copy-start(bf16[2048,32]{0,1:T(8,128)(2,1)} %param.33) | copy-start | bytes 393220
  256.4 74.2 %copy-start.7 = (bf16[2048,32]{0,1:T(8,128)(2,1)S(1)}, bf16[2048,32]{0,1:T(8,128)(2,1)}, u32[]{:S(2)}) copy-start(bf16[2048,32]{0,1:T(8,128)(2,1)} %param.34) | copy-start | bytes 393220
  256.5 93.2 %copy-start.2 = (bf16[512,128]{1,0:T(8,128)(2,1)S(1)}, bf16[512,128]{1,0:T(8,128)(2,1)}, u32[]{:S(2)}) copy-start(bf16[512,128]{1,0:T(8,128)(2,1)} %param.35) | copy-start | bytes 393220
  323.5 24.6 %all-to-all-start.6 = ((bf16[32,1,32,128]{3,2,1,0:T(8,128)(2,1)}), bf16[32,1,32,128]{3,2,1,0:T(8,128)(2,1)S(1)}, u32[]{:S(2)}, u32[]{:S(2)}) async-start(bf16[32,1,32,128]{3,2,1,0:T(8,128)(2,1)} %fusion.8), calls=%async_computation.6 | async-start | bytes 524288 | tf_op jit(solution)/shard_map/all_to_all | solution.py:166
Sparse Core Ops, SparseCore 0:
  256.4 60.4 all-gather.1
